TPU v7x, 32 devices: a whole 2x2x4 slice. The times are simulated.
32 devices in a mesh: fs: 8 (over z, y), tp: 4 (over x, core).
Axes of the slice: x: 2, y: 2, z: 4, core: 2. Of those that a mesh axis runs over, the one named last changes fastest.
Arguments:
- prompt_tokens: bfloat16 [4, 128, 4096], P('tp'), may hold values from -6 to 6
- trained_up: float32 [4096, 16384], P('fs', 'tp'), may hold values from -0.09375 to 0.09375
- trained_down: float32 [16384, 4096], P('fs', 'tp'), may hold values from -0.046875 to 0.046875
- pre_gain: float32 [4096], P('fs'), may hold values from 0.1 to 1.9
- post_gain: float32 [4096], replicated, may hold values from 0.1 to 1.9
Outputs:
- layer_out: bfloat16 [4, 128, 4096], P('tp', 'fs')
- sampler_up: bfloat16 [4096, 16384], P(None, 'fs')
- sampler_down: bfloat16 [16384, 4096], P('fs')
All inputs are finite; a program needn't handle non-finite values.
Results may differ from a plain program's by a relative error of at most 0.0081.
Values may be sent and summed in bfloat16 or wider, within the bound.
A program may use at most 128 MiB of HBM per device.

v0:
```python
import jax
import jax.numpy as jnp
from jax import lax
from jax.sharding import PartitionSpec as P


def row_norm(values):
    return values * lax.rsqrt(jnp.mean(values * values, axis=-1, keepdims=True) + 1e-06)


def on_device(prompt_tokens, trained_up, trained_down, pre_gain, post_gain):
    folded = (pre_gain[:, None] * trained_up).astype(jnp.bfloat16)
    quarter = lax.all_to_all(folded, "tp", split_axis=0, concat_axis=1, tiled=True)
    owned = lax.all_to_all(quarter, "fs", split_axis=1, concat_axis=0, tiled=True)
    joined = lax.all_gather(owned, "tp", axis=0, tiled=True)
    n_fs = lax.axis_size("fs")
    n_tp = lax.axis_size("tp")
    width = joined.shape[1]
    joined = joined.reshape(n_tp, n_fs, joined.shape[0] // (n_tp * n_fs), width)
    sampler_up = jnp.transpose(joined, (1, 0, 2, 3)).reshape(-1, width)
    sampler_down = lax.all_gather(trained_down.astype(jnp.bfloat16), "tp", axis=1, tiled=True)
    flat = prompt_tokens[0].astype(jnp.float32)
    normed = row_norm(flat).astype(jnp.bfloat16)
    upward = jnp.dot(normed, sampler_up, preferred_element_type=jnp.float32)
    hidden = jnp.square(jax.nn.relu(upward)).astype(jnp.bfloat16)
    summed = lax.psum_scatter(
        jnp.dot(hidden, sampler_down, preferred_element_type=jnp.float32),
        "fs",
        scatter_dimension=0,
        tiled=True,
    )
    layer_out = (row_norm(summed) * post_gain).astype(jnp.bfloat16)
    return (layer_out[None], sampler_up, sampler_down)


def solution(mesh):
    placed = (P("tp", None, None), P("fs", "tp"), P("fs", "tp"), P("fs"), P())
    return jax.shard_map(
        on_device,
        mesh=mesh,
        in_specs=placed,
        out_specs=(P("tp", "fs", None), P(None, "fs"), P("fs", None)),
        check_vma=False,
    )
```

profile of v0, /device:TPU:12, one launch (start us, length us, event | category | flops | bytes accessed | tf_op | source)
XLA Modules:
  0.0 495.2 jit_solution(667741849209752609)
XLA Ops:
  7.2 0.0 all-gather.3.cloned.1.call-start
  7.2 4.6 multiply_convert_fusion
  11.8 51.5 %all_to_all.35 = bf16[4,128,4096]{2,1,0:T(8,128)(2,1)} all-to-all(bf16[4,128,4096]{2,1,0:T(8,128)(2,1)S(1)} %bitcast.25), channel_id=1, replica_groups=mesh['fs'=8,'tp'=4] {'tp'}, dimensions={0} | all-to-all | bytes 8388608 | tf_op jit(solution)/shard_map/all_to_all | solution.py:13
  63.4 6.3 %copy.9 = bf16[128,4,4096]{0,2,1:T(8,128)(2,1)} copy(bf16[128,4,4096]{2,0,1:T(8,128)(2,1)} %bitcast.22) | data formatting | bytes 8388608 | tf_op jit(solution)/shard_map/all_to_all | solution.py:13
  69.7 97.0 %all_to_all.36 = bf16[128,8,2048]{0,2,1:T(8,128)(2,1)} all-to-all(bf16[128,8,2048]{0,2,1:T(8,128)(2,1)} %bitcast.23), channel_id=1, replica_groups=mesh['fs'=8,'tp'=4] {'fs'}, dimensions={1} | all-to-all | bytes 8388608 | tf_op jit(solution)/shard_map/all_to_all | solution.py:14
  166.7 6.4 %copy.10 = bf16[8,128,2048]{2,1,0:T(8,128)(2,1)} copy(bf16[8,128,2048]{1,2,0:T(8,128)(2,1)} %bitcast.24) | data formatting | bytes 8388608 | tf_op jit(solution)/shard_map/all_to_all | solution.py:14
  173.1 0.0 all-gather.3.cloned.1.call-update
  173.1 0.0 copy-start
  173.1 0.0 all-gather.5.cloned.1.call-start
  173.2 6.1 %convert_element_type.28 = bf16[2048,1024]{1,0:T(8,128)(2,1)} convert(f32[2048,1024]{1,0:T(8,128)} %param.7) | non-fusion elementwise | flops 2097152 | bytes 12582912 | tf_op jit(solution)/shard_map/convert_element_type | solution.py:21
  179.3 0.0 all-gather.5.cloned.1.call-update
  179.4 0.0 reduce-scatter.2.cloned.1.call-start
  179.4 0.0 copy-done
  179.4 0.3 fusion.2
  179.7 99.5 %all-gather.3.cloned.1.call-done = bf16[4096,2048]{1,0:T(8,128)(2,1)} async-done(((bf16[1024,2048]{1,0:T(8,128)(2,1)}), bf16[4096,2048]{1,0:T(8,128)(2,1)}) %all-gather.3.cloned.1.call-update) | async-done | bytes 16777232 | tf_op jit(solution)/shard_map/all_gather | solution.py:15
  279.2 14.7 %copy.11 = bf16[8,4,128,2048]{3,2,1,0:T(8,128)(2,1)} copy(bf16[8,4,128,2048]{3,2,0,1:T(8,128)(2,1)} %bitcast.20) | data formatting | bytes 33554432 | tf_op jit(solution)/shard_map/transpose | solution.py:20
  293.9 93.3 %all-gather.5.cloned.1.call-done = bf16[2048,4096]{1,0:T(8,128)(2,1)} async-done(((bf16[2048,1024]{1,0:T(8,128)(2,1)}), bf16[2048,4096]{1,0:T(8,128)(2,1)}) %all-gather.5.cloned.1.call-update) | async-done | bytes 16777232 | tf_op jit(solution)/shard_map/all_gather | solution.py:21
  387.2 0.0 copy-start.1
  387.2 16.4 %fusion.8 = f32[128,4096]{1,0:T(8,128)} fusion(bf16[2048,4096]{1,0:T(8,128)(2,1)} %all-gather.5.cloned.1.call-done, bf16[4096,2048]{1,0:T(8,128)(2,1)} %bitcast.18, bf16[1,128,4096]{2,1,0:T(8,128)(2,1)S(1)} %copy-done, f32[128]{0:T(128)S(1)} %add_rsqrt_fusion.1), kind=kOutput, calls=%fused_computation.10 | convolution fusion | flops 4297326592 | bytes 36700672 | tf_op jit(solution)/shard_map/dot_general | solution.py:27
  403.7 0.0 reduce-scatter.2.cloned.1.call-update
  403.7 68.1 %reduce-scatter.2.cloned.1.call-done = f32[16,4096]{1,0:T(8,128)} async-done(((f32[128,4096]{1,0:T(8,128)}), f32[16,4096]{1,0:T(8,128)}) %reduce-scatter.2.cloned.1.call-update) | async-done | bytes 262160 | tf_op jit(solution)/shard_map/reduce_scatter | solution.py:26
  471.8 1.1 multiply_reduce_fusion
  472.9 0.0 copy-done.1
  472.9 1.7 fusion.11
  474.6 14.1 %copy.13 = bf16[2048,4096]{1,0:T(8,128)(2,1)} copy(bf16[2048,4096]{1,0:T(8,128)(2,1)} %all-gather.5.cloned.1.call-done) | data formatting | bytes 33554432
  (2 shorter events, 0.0 us)
Async XLA Ops:
  7.2 272.0 %all-gather.3.cloned.1.call-start = ((), (), s32[]{:S(2)}) async-start(), calls=%async_computation.3 | async-start | bytes 20971520 | tf_op jit(solution)/shard_map/all_gather | solution.py:15
  173.1 6.3 %copy-start = (bf16[1,128,4096]{2,1,0:T(8,128)(2,1)S(1)}, bf16[1,128,4096]{2,1,0:T(8,128)(2,1)}, u32[]{:S(2)}) copy-start(bf16[1,128,4096]{2,1,0:T(8,128)(2,1)} %param.5) | copy-start | bytes 3145732
  173.1 214.1 %all-gather.5.cloned.1.call-start = ((), (), s32[]{:S(2)}) async-start(), calls=%async_computation.4 | async-start | bytes 20971520 | tf_op jit(solution)/shard_map/all_gather | solution.py:21
  179.4 292.4 %reduce-scatter.2.cloned.1.call-start = ((), (), s32[]{:S(2)}) async-start(), calls=%async_computation.5 | async-start | bytes 2359296 | tf_op jit(solution)/shard_map/reduce_scatter | solution.py:26
  387.2 85.6 %copy-start.1 = (f32[4096]{0:T(1024)S(1)}, f32[4096]{0:T(1024)}, u32[]{:S(2)}) copy-start(f32[4096]{0:T(1024)} %param.9) | copy-start | bytes 49156
Sparse Core Ops, SparseCore 0:
  173.2 105.8 all-gather.2
  281.3 105.8 all-gather.4
  403.8 67.8 reduce-scatter.1
where the time goes:
time: 498 us; the launch traced here: 495 us
  waiting for transfers between devices  261 us (52%)
  blocking collectives  149 us (30%)
  local copies, waits for them, and re-layouts  41.5 us (8%)
  matrix products  16.4 us (3%)
  other arithmetic  13.9 us (3%)
  between operations  13.8 us (3%)
    all_gather x1, waiting for transfers between devices, on_device(): joined = lax.all_gather(owned, 'tp', axis=0, tiled=True)  99.5 us
    all_to_all x1, blocking collectives, on_device(): lax.all_to_all(quarter, 'fs', split_axis=1, concat_axis=0, tiled=True)  97 us
    all_gather x1, waiting for transfers between devices, on_device(): lax.all_gather(trained_down.astype(jnp.bfloat16), 'tp', axis=1, tiled=True)  93.3 us
    reduce_scatter x1, waiting for transfers between devices, on_device(): lax.psum_scatter(jnp.dot(hidden, sampler_down, preferred_element_type=jnp...  68.1 us
    all_to_all x1, blocking collectives, on_device(): lax.all_to_all(folded, 'tp', split_axis=0, concat_axis=1, tiled=True)  51.5 us
    dot_general x1, matrix products, on_device(): jnp.dot(hidden, sampler_down, preferred_element_type=jnp.float32)  16.4 us
    transpose x1, local copies, waits for them, and re-layouts, on_device(): sampler_up = jnp.transpose(joined, (1, 0, 2, 3)).reshape(-1, width)  14.7 us
    unnamed x5, local copies, waits for them, and re-layouts  14.1 us
  transfers between devices with their start and end apart: 3, of which 3 were waited for; matrix products, arithmetic and copies ran while one was open for 4% of the time, Pallas kernels for 0%

commit v1 on v0

v1 whole, which is shorter than its diff:
```python
import functools

import jax
import jax.numpy as jnp
from jax import lax
from jax.experimental import pallas as pl
from jax.experimental.pallas import tpu as pltpu
from jax.sharding import PartitionSpec as P

MESH = pl.DeviceIdType.MESH
EPS = 1e-06


def remote(src, dst, send_sem, recv_sem, device):
    return pltpu.make_async_remote_copy(
        src_ref=src, dst_ref=dst, send_sem=send_sem, recv_sem=recv_sem, device_id=device, device_id_type=MESH
    )


def greet(device):
    pl.semaphore_signal(pltpu.get_barrier_semaphore(), inc=1, device_id=device, device_id_type=MESH)


def loop(count, body):
    lax.fori_loop(0, count, lambda i, c: (body(i), c)[1], 0)


def spread_kernel(
    n_fs, n_tp, n_r,
    up, down, gup, gdown, xup,
    xs, xr, ps, pr, ws, wr, ns, nr, ls, ds, dr, vs, vr,
):
    f, t = lax.axis_index("fs"), lax.axis_index("tp")
    far = lax.rem(t + n_tp // 2, n_tp)
    near = t + 1 - 2 * lax.rem(t, 2)
    near_far = lax.rem(near + n_tp // 2, n_tp)
    m = n_fs // n_tp
    rows, width = up.shape[0], up.shape[1] // m
    part = rows // n_r
    d_rows, d_width = down.shape
    d_part = d_rows // n_r
    pieces = m * n_r
    active = lax.rem(lax.rem(f // m, 2) + lax.rem(t, 2), 2) == 0

    def piece(ref, k):
        r, j = k // m, lax.rem(k, m)
        return ref.at[pl.ds(pl.multiple_of(r * part, part), part), pl.ds(pl.multiple_of(j * width, width), width)]

    def landed(source, r):
        return gup.at[pl.ds(pl.multiple_of(source * rows + r * part, part), part), :]

    def x_copy(k):
        return remote(piece(up, k), piece(xup, k), xs.at[k], xr.at[k], {"tp": far})

    def owner(phase, k):
        return (t if phase == 0 else far) * m + lax.rem(k, m)

    def peer_copy(phase, k):
        held = up if phase == 0 else xup
        return remote(piece(held, k), landed(f, k // m), ps.at[phase, k], pr.at[f, k // m], {"fs": owner(phase, k)})

    def start_peer(phase, k):
        mine = owner(phase, k) == f

        @pl.when(mine)
        def _():
            held = up if phase == 0 else xup
            pltpu.make_async_copy(piece(held, k), landed(f, k // m), pr.at[f, k // m]).start()

        @pl.when(jnp.logical_not(mine))
        def _():
            peer_copy(phase, k).start()

    def end_peer(phase, k):
        @pl.when(owner(phase, k) != f)
        def _():
            peer_copy(phase, k).wait_send()

    def block(q, which):
        return gdown.at[
            pl.ds(pl.multiple_of(q * d_part, d_part), d_part), pl.ds(pl.multiple_of(which * d_width, d_width), d_width)
        ]

    def columns(which):
        return gdown.at[:, pl.ds(pl.multiple_of(which * d_width, d_width), d_width)]

    def d_copy(q):
        return remote(
            down.at[pl.ds(pl.multiple_of(q * d_part, d_part), d_part), :], block(q, t), ds.at[q], dr.at[q], {"tp": far}
        )

    def d_pass(q, which):
        return remote(block(q, which), block(q, which), vs.at[q], vr.at[q], {"tp": near})

    def share(source, r):
        return remote(landed(source, r), landed(source, r), ws.at[source, r], wr.at[source, r], {"tp": near})

    loop(n_fs - 1, lambda i: greet({"fs": lax.rem(f + 1 + i, n_fs)}))
    greet({"tp": far})
    greet({"tp": near})
    pl.semaphore_wait(pltpu.get_barrier_semaphore(), n_fs + 1)

    loop(pieces, lambda k: x_copy(k).start())
    loop(pieces, lambda k: start_peer(0, k))
    to_near = remote(down, columns(t), ns, nr, {"tp": near})
    to_near.start()
    own = pltpu.make_async_copy(down, columns(t), ls)
    own.start()

    def pass_on(k):
        @pl.when(k == pieces - 1)
        def _():
            loop(n_r, lambda q: d_copy(q).start())

        x_copy(k).wait_recv()
        start_peer(1, k)

    loop(pieces, pass_on)

    def gather(r):
        @pl.when(active)
        def _():
            def one(source):
                @pl.when(source == f)
                def _():
                    pltpu.make_async_copy(landed(f, r), landed(f, r), pr.at[f, r]).wait()

                @pl.when(source != f)
                def _():
                    remote(landed(source, r), landed(source, r), ws.at[source, r], pr.at[source, r], {"tp": near}).wait_recv()

                share(source, r).start()

            loop(n_fs, one)

        remote(block(r, far), block(r, far), ds.at[r], dr.at[r], {"tp": far}).wait_recv()
        d_pass(r, far).start()

    loop(n_r, gather)

    def ended(i):
        source, r = i // n_r, lax.rem(i, n_r)

        @pl.when(active)
        def _():
            share(source, r).wait_send()

        @pl.when(jnp.logical_not(active))
        def _():
            share(source, r).wait_recv()

    loop(n_fs * n_r, ended)
    own.wait()
    to_near.wait_send()
    remote(columns(near), columns(near), ns, nr, {"tp": near}).wait_recv()

    def ended_down(q):
        d_copy(q).wait_send()
        d_pass(q, far).wait_send()
        d_pass(q, near_far).wait_recv()

    loop(n_r, ended_down)

    def ended_pieces(k):
        x_copy(k).wait_send()
        end_peer(0, k)
        end_peer(1, k)

    loop(pieces, ended_pieces)


def layer_kernel(tokens, up, down, part_out, up_out, down_out, normed, total):
    step = pl.program_id(0)

    @pl.when(step == 0)
    def _():
        flat = tokens[...].astype(jnp.float32)
        normed[...] = (flat * lax.rsqrt(jnp.mean(flat * flat, axis=-1, keepdims=True) + EPS)).astype(jnp.bfloat16)
        total[...] = jnp.zeros_like(total)

    up_out[...] = up[...]
    down_out[...] = down[...]
    upward = jnp.dot(normed[...], up[...], preferred_element_type=jnp.float32)
    hidden = jnp.square(jnp.maximum(upward, 0.0)).astype(jnp.bfloat16)
    total[...] += jnp.dot(hidden, down[...], preferred_element_type=jnp.float32)

    @pl.when(step == pl.num_programs(0) - 1)
    def _():
        part_out[...] = total[...].astype(part_out.dtype)


def sum_kernel(n_fs, parts, gain, out, land, ss, rs):
    f = lax.axis_index("fs")

    def peer_of(i):
        return lax.rem(f + 1 + i, n_fs)

    loop(n_fs - 1, lambda i: greet({"fs": peer_of(i)}))
    pl.semaphore_wait(pltpu.get_barrier_semaphore(), n_fs - 1)

    def send(i):
        return remote(parts.at[peer_of(i)], land.at[f], ss.at[i], rs.at[f], {"fs": peer_of(i)})

    loop(n_fs - 1, lambda i: send(i).start())

    def add(i, total):
        source = peer_of(i)
        remote(land.at[source], land.at[source], ss.at[i], rs.at[source], {"fs": source}).wait_recv()
        return total + land[source].astype(jnp.float32)

    summed = lax.fori_loop(0, n_fs - 1, add, parts[f].astype(jnp.float32))
    scale = lax.rsqrt(jnp.mean(summed * summed, axis=-1, keepdims=True) + EPS)
    out[...] = (summed * scale * gain[...]).astype(out.dtype)
    loop(n_fs - 1, lambda i: send(i).wait_send())


def on_device(n_fs, n_tp, prompt_tokens, trained_up, trained_down, pre_gain, post_gain):
    bf16 = jnp.bfloat16
    up = (pre_gain[:, None] * trained_up).astype(bf16)
    down = trained_down.astype(bf16)
    rows, cols = up.shape
    d_rows, d_cols = down.shape
    tokens, width = prompt_tokens.shape[1:]
    m = n_fs // n_tp
    owned = cols // m
    n_r = max(1, rows // 128)
    pieces = m * n_r
    anywhere = pl.BlockSpec(memory_space=pl.ANY)
    vmem = pl.BlockSpec(memory_space=pltpu.VMEM)
    dma = pltpu.SemaphoreType.DMA
    gup, gdown = pl.pallas_call(
        functools.partial(spread_kernel, n_fs, n_tp, n_r),
        out_shape=(
            jax.ShapeDtypeStruct((n_fs * rows, owned), bf16),
            jax.ShapeDtypeStruct((d_rows, n_tp * d_cols), bf16),
        ),
        in_specs=[vmem, vmem],
        out_specs=(anywhere, anywhere),
        scratch_shapes=[
            pltpu.VMEM(up.shape, bf16),
            dma((pieces,)), dma((pieces,)),
            dma((2, pieces)), dma((n_fs, n_r)),
            dma((n_fs, n_r)), dma((n_fs, n_r)),
            dma, dma, dma,
            dma((n_r,)), dma((n_r,)),
            dma((n_r,)), dma((n_r,)),
        ],
        compiler_params=pltpu.CompilerParams(collective_id=0, has_side_effects=True),
    )(up, down)

    tile = min(owned, 256)
    parts, sampler_up, sampler_down = pl.pallas_call(
        layer_kernel,
        grid=(owned // tile,),
        out_shape=(
            jax.ShapeDtypeStruct((tokens, width), bf16),
            jax.ShapeDtypeStruct(gup.shape, bf16),
            jax.ShapeDtypeStruct(gdown.shape, bf16),
        ),
        in_specs=[
            pl.BlockSpec((tokens, width), lambda i: (0, 0)),
            pl.BlockSpec((gup.shape[0], tile), lambda i: (0, i)),
            pl.BlockSpec((tile, gdown.shape[1]), lambda i: (i, 0)),
        ],
        out_specs=(
            pl.BlockSpec((tokens, width), lambda i: (0, 0)),
            pl.BlockSpec((gup.shape[0], tile), lambda i: (0, i)),
            pl.BlockSpec((tile, gdown.shape[1]), lambda i: (i, 0)),
        ),
        scratch_shapes=[pltpu.VMEM((tokens, width), bf16), pltpu.VMEM((tokens, width), jnp.float32)],
    )(prompt_tokens[0], gup, gdown)

    share = tokens // n_fs
    layer_out = pl.pallas_call(
        functools.partial(sum_kernel, n_fs),
        out_shape=jax.ShapeDtypeStruct((share, width), bf16),
        in_specs=[vmem, vmem],
        out_specs=vmem,
        scratch_shapes=[pltpu.VMEM((n_fs, share, width), bf16), dma((n_fs - 1,)), dma((n_fs,))],
        compiler_params=pltpu.CompilerParams(collective_id=1, has_side_effects=True),
    )(parts.reshape(n_fs, share, width), post_gain[None])
    return (layer_out[None], sampler_up, sampler_down)


def solution(mesh):
    placed = (P("tp", None, None), P("fs", "tp"), P("fs", "tp"), P("fs"), P())
    return jax.shard_map(
        functools.partial(on_device, mesh.shape["fs"], mesh.shape["tp"]),
        mesh=mesh,
        in_specs=placed,
        out_specs=(P("tp", "fs", None), P(None, "fs"), P("fs", None)),
        check_vma=False,
    )
```

time: 498 us -> 279 us (0.56)
  Pallas kernels: 0 us -> 267 us
  waiting for transfers between devices: 261 us -> 0 us
  blocking collectives: 149 us -> 0 us
  local copies, waits for them, and re-layouts: 41.5 us -> 1.57 us
  matrix products: 16.4 us -> 0 us
  between operations: 13.8 us -> 0.66 us
    pallas_call x0 -> x3, Pallas kernels: none -> 267 us  [the longest x1 200 us: on_device(): pl.pallas_call(functools.partial(spread_kernel, n_fs, n_tp, n_r), out_sha...]
    all_gather x2 -> x0, waiting for transfers between devices: 193 us -> none  [the longest x1 99.5 us: on_device(): joined = lax.all_gather(owned, 'tp', axis=0, tiled=True)]
    all_to_all x2 -> x0, blocking collectives: 149 us -> none  [the longest x1 97 us: on_device(): lax.all_to_all(quarter, 'fs', split_axis=1, concat_axis=0, tiled=True)]
    reduce_scatter x1 -> x0, waiting for transfers between devices: 68.1 us -> none  [on_device(): lax.psum_scatter(jnp.dot(hidden, sampler_down, preferred_element_type=jnp...]
    dot_general x1 -> x0, matrix products: 16.4 us -> none  [on_device(): jnp.dot(hidden, sampler_down, preferred_element_type=jnp.float32)]
    transpose x1 -> x0, local copies, waits for them, and re-layouts: 14.7 us -> none  [on_device(): sampler_up = jnp.transpose(joined, (1, 0, 2, 3)).reshape(-1, width)]
    all_to_all x2 -> x0, local copies, waits for them, and re-layouts: 12.7 us -> none  [the longest x1 6.43 us: on_device(): lax.all_to_all(quarter, 'fs', split_axis=1, concat_axis=0, tiled=True)]
    unnamed x5 -> x3, local copies, waits for them, and re-layouts: 14.1 us -> 1.57 us
  transfers between devices with their start and end apart: 3 -> 0, of which waited for: 3 -> 0; matrix products, arithmetic and copies ran while one was open for 4% -> 0% of each run, Pallas kernels for 0% -> 0%
where the time goes in v1:
time: 279 us
  Pallas kernels  267 us (96%)
  other arithmetic  9.48 us (3%)
    pallas_call x1, Pallas kernels, on_device(): pl.pallas_call(functools.partial(spread_kernel, n_fs, n_tp, n_r), out_sha...  200 us
    pallas_call x1, Pallas kernels, on_device(): pl.pallas_call(functools.partial(sum_kernel, n_fs), out_shape=jax.ShapeDt...  38.1 us
    pallas_call x1, Pallas kernels, on_device(): pl.pallas_call(layer_kernel, grid=(owned // tile,), out_shape=(jax.ShapeD...  29.6 us
    convert_element_type x1, other arithmetic, on_device(): up = (pre_gain[:, None] * trained_up).astype(bf16)  6.81 us

profile of v1, /device:TPU:12, one launch (start us, length us, event | category | flops | bytes accessed | tf_op | source)
XLA Modules:
  0.0 279.1 jit_solution(10735970211720748919)
XLA Ops:
  0.6 0.0 copy-start
  0.6 6.8 %multiply_convert_fusion.up = bf16[512,4096]{1,0:T(8,128)(2,1)} fusion(f32[512,4096]{1,0:T(8,128)} %param.6, f32[512]{0:T(512)} %param.8), kind=kLoop, calls=%fused_computation | loop fusion | flops 4194304 | bytes 12584960 | tf_op jit(solution)/shard_map/convert_element_type | solution.py:219
  7.5 0.0 copy-done
  7.5 2.7 convert_element_type.7.down
  10.1 199.7 %shard_map.76 = (bf16[4096,2048]{1,0:T(8,128)(2,1)}, bf16[2048,4096]{1,0:T(8,128)(2,1)}) custom-call(bf16[512,4096]{1,0:T(8,128)(2,1)} %multiply_convert_fusion.up, bf16[2048,1024]{1,0:T(8,128)(2,1)} %convert_element_type.7.down), custom_call_target="tpu_custom_call" | custom-call | tf_op jit(solution)/shard_map/pallas_call | solution.py:231
  209.9 29.6 %shard_map.77 = (bf16[128,4096]{1,0:T(8,128)(2,1)}, bf16[4096,2048]{1,0:T(8,128)(2,1)}, bf16[2048,4096]{1,0:T(8,128)(2,1)}) custom-call(bf16[128,4096]{1,0:T(8,128)(2,1)} %bitcast.4, bf16[4096,2048]{1,0:T(8,128)(2,1)} %get-tuple-element.8.up, bf16[2048,4096]{1,0:T(8,128)(2,1)} %get-tuple-element.9.down), custom_call_target="tpu_custom_call" | custom-call | tf_op jit(solution)/shard_map/pallas_call | solution.py:252
  239.4 38.1 %shard_map.78 = bf16[16,4096]{1,0:T(8,128)(2,1)} custom-call(bf16[8,16,4096]{2,1,0:T(8,128)(2,1)} %bitcast.5, f32[1,4096]{1,0:T(1,128)} %bitcast.7), custom_call_target="tpu_custom_call" | custom-call | tf_op jit(solution)/shard_map/pallas_call | solution.py:274
  277.6 1.6 copy.9
Async XLA Ops:
  0.6 6.8 %copy-start = (f32[2048,1024]{1,0:T(8,128)S(1)}, f32[2048,1024]{1,0:T(8,128)}, u32[]{:S(2)}) copy-start(f32[2048,1024]{1,0:T(8,128)} %param.7) | copy-start | bytes 25165828

commit v2 on v1

v2 whole, which is shorter than its diff:
```python
import functools

import jax
import jax.numpy as jnp
from jax import lax
from jax.experimental import pallas as pl
from jax.experimental.pallas import tpu as pltpu
from jax.sharding import PartitionSpec as P

MESH = pl.DeviceIdType.MESH
EPS = 1e-06


def remote(src, dst, send_sem, recv_sem, device):
    return pltpu.make_async_remote_copy(
        src_ref=src, dst_ref=dst, send_sem=send_sem, recv_sem=recv_sem, device_id=device, device_id_type=MESH
    )


def greet(device):
    pl.semaphore_signal(pltpu.get_barrier_semaphore(), inc=1, device_id=device, device_id_type=MESH)


def loop(count, body):
    lax.fori_loop(0, count, lambda i, c: (body(i), c)[1], 0)


def spread_kernel(
    n_fs, n_tp, n_r,
    up, down, tokens, gup, gdown, parts, held_up, held_down, xup, normed, upward, hidden,
    xs, xr, ps, pr, ws, wr, ns, nr, us, ls, ds, dr, vs, vr,
):
    f, t = lax.axis_index("fs"), lax.axis_index("tp")
    far = lax.rem(t + n_tp // 2, n_tp)
    near = t + 1 - 2 * lax.rem(t, 2)
    near_far = lax.rem(near + n_tp // 2, n_tp)
    m = n_fs // n_tp
    rows, width = up.shape[0], up.shape[1] // m
    part = rows // n_r
    d_rows, d_width = down.shape
    d_part = d_rows // n_r
    pieces = m * n_r
    block_of_f = f // m
    active = lax.rem(lax.rem(block_of_f, 2) + lax.rem(t, 2), 2) == 0

    def piece_at(r, j):
        return (
            pl.ds(pl.multiple_of(r * part, part), part),
            pl.ds(pl.multiple_of(j * width, width), width),
        )

    def piece(ref, k):
        return ref.at[piece_at(k // m, lax.rem(k, m))]

    def rows_of(source, r):
        return pl.ds(pl.multiple_of(source * rows + r * part, part), part)

    def landed(source, r):
        return held_up.at[rows_of(source, r)]

    def x_copy(k):
        return remote(piece(up, k), piece(xup, k), xs.at[k], xr.at[k], {"tp": far})

    def owner(phase, k):
        return (t if phase == 0 else far) * m + lax.rem(k, m)

    def peer_copy(phase, k):
        held = up if phase == 0 else xup
        return remote(piece(held, k), landed(f, k // m), ps.at[phase, k], pr.at[f, k // m], {"fs": owner(phase, k)})

    def start_peer(phase, k):
        @pl.when(owner(phase, k) != f)
        def _():
            peer_copy(phase, k).start()

    def end_peer(phase, k):
        @pl.when(owner(phase, k) != f)
        def _():
            peer_copy(phase, k).wait_send()

    def d_rows_of(q):
        return pl.ds(pl.multiple_of(q * d_part, d_part), d_part)

    def columns(which):
        return pl.ds(pl.multiple_of(which * d_width, d_width), d_width)

    def block(q, which):
        return held_down.at[which, d_rows_of(q)]

    def d_copy(q):
        return remote(down.at[d_rows_of(q)], block(q, t), ds.at[q], dr.at[q], {"tp": far})

    def d_pass(q, which):
        return remote(block(q, which), block(q, which), vs.at[q], vr.at[q], {"tp": near})

    def d_put(q, which):
        pltpu.make_async_copy(block(q, which), gdown.at[d_rows_of(q), columns(which)], ls).start()

    def share(src, source, r):
        return remote(src, landed(source, r), ws.at[source, r], wr.at[source, r], {"tp": near})

    def put(src, source, r):
        pltpu.make_async_copy(src, gup.at[rows_of(source, r)], us).start()

    loop(n_fs - 1, lambda i: greet({"fs": lax.rem(f + 1 + i, n_fs)}))
    greet({"tp": far})
    greet({"tp": near})
    pl.semaphore_wait(pltpu.get_barrier_semaphore(), n_fs + 1)

    loop(pieces, lambda k: x_copy(k).start())
    loop(pieces, lambda k: start_peer(0, k))
    to_near = remote(down, held_down.at[t], ns, nr, {"tp": near})
    to_near.start()
    pltpu.make_async_copy(down, gdown.at[:, columns(t)], ls).start()

    flat = tokens[...].astype(jnp.float32)
    scaled = (flat * lax.rsqrt(jnp.mean(flat * flat, axis=-1, keepdims=True) + EPS)).astype(jnp.bfloat16)
    for i in range(n_fs * n_r):
        normed[i] = scaled[:, i * part : (i + 1) * part]
    upward[...] = jnp.zeros_like(upward)

    def keep_down(q):
        held_down[t, d_rows_of(q)] = down[d_rows_of(q)]

    loop(n_r, keep_down)

    def pass_on(k):
        @pl.when(k == pieces - 1)
        def _():
            loop(n_r, lambda q: d_copy(q).start())

        x_copy(k).wait_recv()
        start_peer(1, k)

    loop(pieces, pass_on)

    def gather(r):
        def one(source):
            def keep_own(held):
                src = held.at[piece_at(r, lax.rem(f, m))]
                share(src, source, r).start()
                put(src, source, r)
                held_up[rows_of(source, r)] = held[piece_at(r, lax.rem(f, m))]

            @pl.when(jnp.logical_and(active, source == f))
            def _():
                @pl.when(block_of_f == t)
                def _():
                    keep_own(up)

                @pl.when(block_of_f != t)
                def _():
                    keep_own(xup)

            @pl.when(jnp.logical_and(active, source != f))
            def _():
                remote(landed(source, r), landed(source, r), ws.at[source, r], pr.at[source, r], {"tp": near}).wait_recv()
                share(landed(source, r), source, r).start()
                put(landed(source, r), source, r)

            @pl.when(jnp.logical_not(active))
            def _():
                share(landed(source, r), source, r).wait_recv()
                put(landed(source, r), source, r)

            upward[...] += jnp.dot(
                normed[source * n_r + r], held_up[rows_of(source, r)], preferred_element_type=jnp.float32
            )

        loop(n_fs, one)
        remote(block(r, far), block(r, far), ds.at[r], dr.at[r], {"tp": far}).wait_recv()
        d_pass(r, far).start()
        d_put(r, far)
        d_pass(r, near_far).wait_recv()
        d_put(r, near_far)

    loop(n_r, gather)
    remote(held_down.at[near], held_down.at[near], ns, nr, {"tp": near}).wait_recv()
    pltpu.make_async_copy(held_down.at[near], gdown.at[:, columns(near)], ls).start()

    hidden[...] = jnp.square(jnp.maximum(upward[...], 0.0)).astype(jnp.bfloat16)
    tile = min(d_width, 256)
    per_block = d_width // tile

    def finish(i):
        b, j = i // per_block, lax.rem(i, per_block)
        parts[:, pl.ds(pl.multiple_of(i * tile, tile), tile)] = jnp.dot(
            hidden[...],
            held_down[b, :, pl.ds(pl.multiple_of(j * tile, tile), tile)],
            preferred_element_type=jnp.float32,
        ).astype(parts.dtype)

    loop(n_tp * per_block, finish)

    def ended(i):
        @pl.when(active)
        def _():
            source, r = i // n_r, lax.rem(i, n_r)
            share(landed(source, r), source, r).wait_send()

    loop(n_fs * n_r, ended)
    to_near.wait_send()

    def ended_down(q):
        d_copy(q).wait_send()
        d_pass(q, far).wait_send()

    loop(n_r, ended_down)

    def ended_pieces(k):
        x_copy(k).wait_send()
        end_peer(0, k)
        end_peer(1, k)

    loop(pieces, ended_pieces)
    pltpu.make_async_copy(held_up, gup, us).wait()
    pltpu.make_async_copy(gdown, gdown, ls).wait()


def copy_kernel(up, down, up_out, down_out):
    up_out[...] = up[...]
    down_out[...] = down[...]


def sum_kernel(n_fs, parts, gain, out, land, ss, rs):
    f = lax.axis_index("fs")

    def peer_of(i):
        return lax.rem(f + 1 + i, n_fs)

    loop(n_fs - 1, lambda i: greet({"fs": peer_of(i)}))
    pl.semaphore_wait(pltpu.get_barrier_semaphore(), n_fs - 1)

    def send(i):
        return remote(parts.at[peer_of(i)], land.at[f], ss.at[i], rs.at[f], {"fs": peer_of(i)})

    loop(n_fs - 1, lambda i: send(i).start())

    def add(i, total):
        source = peer_of(i)
        remote(land.at[source], land.at[source], ss.at[i], rs.at[source], {"fs": source}).wait_recv()
        return total + land[source].astype(jnp.float32)

    summed = lax.fori_loop(0, n_fs - 1, add, parts[f].astype(jnp.float32))
    scale = lax.rsqrt(jnp.mean(summed * summed, axis=-1, keepdims=True) + EPS)
    out[...] = (summed * scale * gain[...]).astype(out.dtype)
    loop(n_fs - 1, lambda i: send(i).wait_send())


def on_device(n_fs, n_tp, prompt_tokens, trained_up, trained_down, pre_gain, post_gain):
    bf16 = jnp.bfloat16
    up = (pre_gain[:, None] * trained_up).astype(bf16)
    down = trained_down.astype(bf16)
    rows, cols = up.shape
    d_rows, d_cols = down.shape
    tokens, width = prompt_tokens.shape[1:]
    m = n_fs // n_tp
    owned = cols // m
    n_r = max(1, rows // 128)
    pieces = m * n_r
    anywhere = pl.BlockSpec(memory_space=pl.ANY)
    vmem = pl.BlockSpec(memory_space=pltpu.VMEM)
    dma = pltpu.SemaphoreType.DMA
    gup, gdown, parts = pl.pallas_call(
        functools.partial(spread_kernel, n_fs, n_tp, n_r),
        out_shape=(
            jax.ShapeDtypeStruct((n_fs * rows, owned), bf16),
            jax.ShapeDtypeStruct((d_rows, n_tp * d_cols), bf16),
            jax.ShapeDtypeStruct((tokens, width), bf16),
        ),
        in_specs=[vmem, vmem, vmem],
        out_specs=(anywhere, anywhere, vmem),
        scratch_shapes=[
            pltpu.VMEM((n_fs * rows, owned), bf16),
            pltpu.VMEM((n_tp, d_rows, d_cols), bf16),
            pltpu.VMEM(up.shape, bf16),
            pltpu.VMEM((n_fs * n_r, tokens, rows // n_r), bf16),
            pltpu.VMEM((tokens, owned), jnp.float32),
            pltpu.VMEM((tokens, owned), bf16),
            dma((pieces,)), dma((pieces,)),
            dma((2, pieces)), dma((n_fs, n_r)),
            dma((n_fs, n_r)), dma((n_fs, n_r)),
            dma, dma, dma, dma,
            dma((n_r,)), dma((n_r,)),
            dma((n_r,)), dma((n_r,)),
        ],
        compiler_params=pltpu.CompilerParams(collective_id=0, has_side_effects=True, vmem_limit_bytes=64000000),
    )(up, down, prompt_tokens[0])

    steps = 8
    blocks = [
        pl.BlockSpec((gup.shape[0] // steps, owned), lambda i: (i, 0)),
        pl.BlockSpec((d_rows // steps, gdown.shape[1]), lambda i: (i, 0)),
    ]
    sampler_up, sampler_down = pl.pallas_call(
        copy_kernel,
        grid=(steps,),
        out_shape=(jax.ShapeDtypeStruct(gup.shape, bf16), jax.ShapeDtypeStruct(gdown.shape, bf16)),
        in_specs=blocks,
        out_specs=tuple(blocks),
    )(gup, gdown)

    share = tokens // n_fs
    layer_out = pl.pallas_call(
        functools.partial(sum_kernel, n_fs),
        out_shape=jax.ShapeDtypeStruct((share, width), bf16),
        in_specs=[vmem, vmem],
        out_specs=vmem,
        scratch_shapes=[pltpu.VMEM((n_fs, share, width), bf16), dma((n_fs - 1,)), dma((n_fs,))],
        compiler_params=pltpu.CompilerParams(collective_id=1, has_side_effects=True),
    )(parts.reshape(n_fs, share, width), post_gain[None])
    return (layer_out[None], sampler_up, sampler_down)


def solution(mesh):
    placed = (P("tp", None, None), P("fs", "tp"), P("fs", "tp"), P("fs"), P())
    return jax.shard_map(
        functools.partial(on_device, mesh.shape["fs"], mesh.shape["tp"]),
        mesh=mesh,
        in_specs=placed,
        out_specs=(P("tp", "fs", None), P(None, "fs"), P("fs", None)),
        check_vma=False,
    )
```

time: 279 us -> 278 us (level)
    pallas_call x1, Pallas kernels: 29.6 us -> 22.6 us  [on_device(): pl.pallas_call(copy_kernel, grid=(steps,), out_shape=(jax.ShapeDtypeStruc...]
    pallas_call x1, Pallas kernels: 38.1 us -> 43.5 us  [on_device(): pl.pallas_call(functools.partial(sum_kernel, n_fs), out_shape=jax.ShapeDt...]
where the time goes in v2:
time: 278 us
  Pallas kernels  267 us (96%)
  other arithmetic  9.49 us (3%)
    pallas_call x1, Pallas kernels, on_device(): pl.pallas_call(functools.partial(spread_kernel, n_fs, n_tp, n_r), out_sha...  201 us
    pallas_call x1, Pallas kernels, on_device(): pl.pallas_call(functools.partial(sum_kernel, n_fs), out_shape=jax.ShapeDt...  43.5 us
    pallas_call x1, Pallas kernels, on_device(): pl.pallas_call(copy_kernel, grid=(steps,), out_shape=(jax.ShapeDtypeStruc...  22.6 us
    convert_element_type x1, other arithmetic, on_device(): up = (pre_gain[:, None] * trained_up).astype(bf16)  6.81 us

profile of v2, /device:TPU:12, one launch (start us, length us, event | category | flops | bytes accessed | tf_op | source)
XLA Modules:
  0.0 278.1 jit_solution(11021396355126294380)
XLA Ops:
  0.6 0.0 copy-start
  0.6 6.8 %multiply_convert_fusion.up = bf16[512,4096]{1,0:T(8,128)(2,1)} fusion(f32[512,4096]{1,0:T(8,128)} %param.6, f32[512]{0:T(512)} %param.8), kind=kLoop, calls=%fused_computation | loop fusion | flops 4194304 | bytes 12584960 | tf_op jit(solution)/shard_map/convert_element_type | solution.py:252
  7.5 0.0 copy-done
  7.5 2.7 convert_element_type.7.down
  10.1 201.2 %shard_map.76 = (bf16[4096,2048]{1,0:T(8,128)(2,1)}, bf16[2048,4096]{1,0:T(8,128)(2,1)}, bf16[128,4096]{1,0:T(8,128)(2,1)}) custom-call(bf16[512,4096]{1,0:T(8,128)(2,1)} %multiply_convert_fusion.up, bf16[2048,1024]{1,0:T(8,128)(2,1)} %convert_element_type.7.down, bf16[128,4096]{1,0:T(8,128)(2,1)} %bitcast.4), custom_call_target="tpu_custom_call" | custom-call | tf_op jit(solution)/shard_map/pallas_call | solution.py:264
  211.3 43.5 %shard_map.77 = bf16[16,4096]{1,0:T(8,128)(2,1)} custom-call(bf16[8,16,4096]{2,1,0:T(8,128)(2,1)} %bitcast.5, f32[1,4096]{1,0:T(1,128)} %bitcast.7), custom_call_target="tpu_custom_call" | custom-call | tf_op jit(solution)/shard_map/pallas_call | solution.py:304
  254.8 0.0 copy-start.1
  254.8 22.6 %shard_map.78 = (bf16[4096,2048]{1,0:T(8,128)(2,1)}, bf16[2048,4096]{1,0:T(8,128)(2,1)}) custom-call(bf16[4096,2048]{1,0:T(8,128)(2,1)} %get-tuple-element.9.up, bf16[2048,4096]{1,0:T(8,128)(2,1)} %get-tuple-element.10.down), custom_call_target="tpu_custom_call" | custom-call | tf_op jit(solution)/shard_map/pallas_call | solution.py:295
  277.4 0.0 copy-done.1
  277.4 0.7 copy.9
Async XLA Ops:
  0.6 6.8 %copy-start = (f32[2048,1024]{1,0:T(8,128)S(1)}, f32[2048,1024]{1,0:T(8,128)}, u32[]{:S(2)}) copy-start(f32[2048,1024]{1,0:T(8,128)} %param.7) | copy-start | bytes 25165828
  254.8 22.6 %copy-start.1 = (bf16[16,4096]{1,0:T(8,128)(2,1)S(1)}, bf16[16,4096]{1,0:T(8,128)(2,1)}, u32[]{:S(2)}) copy-start(bf16[16,4096]{1,0:T(8,128)(2,1)} %shard_map.77) | copy-start | bytes 393220
